TPU v7x, 256 devices: a 4x2x16 block of a 4x16x16 slice. The times are simulated.
256 devices in a mesh: grp: 2 (over y), sp: 32 (over z, core), tp: 4 (over x).
Axes of the slice: x: 4, y: 2, z: 16, core: 2. Of those that a mesh axis runs over, the one named last changes fastest.
The devices are a block of a 4x16x16 slice.
Arguments:
- queries: bfloat16 [8192, 512], P(('grp', 'sp'), 'tp'), parts along dimension 0, may hold values from -6 to 6
- key_rows: bfloat16 [8192, 512], P(('grp', 'sp'), 'tp'), parts along dimension 0, may hold values from -6 to 6
- value_rows: bfloat16 [8192, 512], P(('grp', 'sp'), 'tp'), parts along dimension 0, may hold values from -16 to 16
- key_bias: bfloat16 [8, 8192], P('tp', ('grp', 'sp')), parts along dimension 1, may hold values from -20 to 0
- residual: bfloat16 [8192, 2048], P(('grp', 'sp')), parts along dimension 0, may hold values from -6 to 6
- out_weight: bfloat16 [512, 2048], P('tp'), may hold values from -0.25 to 0.25
- norm_gain: bfloat16 [2048], replicated, may hold values from 0.099609375 to 1.8984375
- gate_weight: bfloat16 [2048, 3072], P('sp', 'tp'), may hold values from -0.125 to 0.125
- up_weight: bfloat16 [2048, 3072], P('sp', 'tp'), may hold values from -0.125 to 0.125
- down_weight: bfloat16 [3072, 2048], P('tp', 'sp'), may hold values from -0.109375 to 0.109375
Outputs:
- layer_out: bfloat16 [8192, 2048], P(('grp', 'sp')), parts along dimension 0
There are 2 independent parts, one for each index of `grp`. A program takes and returns all parts, laid end to end along the dimension named above; an argument that names none is the same for every part. Nothing has to cross between parts.
All inputs are finite; a program needn't handle non-finite values.
Results may differ from a plain program's by a relative error of at most 0.014.
Values may be sent and summed in bfloat16 or wider, within the bound.
No kernel may reach another device: no remote copies, remote signals or barrier semaphores. Data moves between devices by JAX's collectives and lax.ppermute only.
A program may use at most 64 MiB of HBM per device.

v0:
```python
import jax
import jax.numpy as jnp
from jax import lax
from jax.sharding import PartitionSpec as P

norm_eps = 1e-05


def side_by_side(arrays, axis, dim, along):
    both = jnp.concatenate(arrays, axis=along)
    out, at, done = (lax.all_gather(both, axis, axis=dim, tiled=True), 0, [])
    for a in arrays:
        done.append(lax.slice_in_dim(out, at, at + a.shape[along], axis=along))
        at += a.shape[along]
    return tuple(done)


def turned_gather(arrays, axis, dims):
    turned = [jnp.moveaxis(a, dim, 0) for a, dim in zip(arrays, dims)]
    widths = [t[0].size for t in turned]
    both = jnp.concatenate([t.reshape(-1, w) for t, w in zip(turned, widths)], axis=1)
    out = lax.all_gather(both, axis, axis=0, tiled=True)
    blocks = jnp.split(out, [sum(widths[:k]) for k in range(1, len(widths))], axis=1)
    return tuple(
        (
            jnp.moveaxis(b.reshape(-1, *t.shape[1:]), 0, dim)
            for b, t, dim in zip(blocks, turned, dims)
        )
    )


def cut_along(value, dim, length):
    shape = value.shape
    blocks = value.reshape(*shape[:dim], length, shape[dim] // length, *shape[dim + 1 :])
    return jnp.moveaxis(blocks, dim, 0)


def sum_at_owner(value, axis, dim):
    length = lax.axis_size(axis)
    blocks = lax.all_to_all(cut_along(value, dim, length), axis, 0, 0, tiled=True)
    return jnp.sum(blocks.astype(jnp.float32), axis=0)


def in_order(blocks, dim):
    blocks = jnp.moveaxis(blocks, 0, dim)
    shape = blocks.shape
    return blocks.reshape(*shape[:dim], shape[dim] * shape[dim + 1], *shape[dim + 2 :])


def sent_to_all(value, axis):
    copies = jnp.broadcast_to(value, (lax.axis_size(axis), *value.shape))
    return lax.all_to_all(copies, axis, split_axis=0, concat_axis=0, tiled=True)


def collect(value, axis, dim):
    return in_order(sent_to_all(value, axis), dim)


def stick_block(carry, query_heads, key_block, value_block, bias_block, query_pos, key_start):
    accum, kept_log = carry
    key_count = key_block.shape[0]
    head_count = query_heads.shape[1]
    key_heads = key_block.reshape(key_count, head_count, -1)
    value_heads = value_block.reshape(key_count, head_count, -1)
    scale = key_heads.shape[2] ** (-0.5)
    scores = (
        jnp.einsum("qhd,khd->hqk", query_heads, key_heads, preferred_element_type=jnp.float32)
        * scale
    )
    scores = scores + bias_block.astype(jnp.float32)[:, None, :]
    key_pos = key_start + lax.iota(jnp.int32, key_count)
    strict = ((key_pos[None, :] < query_pos[:, None]) & (key_pos[None, :] >= 0))[None]
    log_retained = jnp.where(strict, jax.nn.log_sigmoid(-scores), 0.0)
    between = lax.cumsum(log_retained, axis=2, reverse=True) - log_retained + kept_log[:, :, None]
    stick = jnp.where(strict, jnp.exp(jax.nn.log_sigmoid(scores) + between), 0.0).astype(
        jnp.bfloat16
    )
    accum = accum + jnp.einsum(
        "hqk,khd->qhd", stick, value_heads, preferred_element_type=jnp.float32
    )
    return (accum, kept_log + jnp.sum(log_retained, axis=2))


def normalize(middle_wide, norm_gain):
    mean_square = jnp.mean(middle_wide * middle_wide, axis=1, keepdims=True)
    return (middle_wide * lax.rsqrt(mean_square + norm_eps) * norm_gain.astype(jnp.float32)).astype(
        jnp.bfloat16
    )


def body(
    queries,
    key_rows,
    value_rows,
    key_bias,
    residual,
    out_weight,
    norm_gain,
    gate_weight,
    up_weight,
    down_weight,
):
    gate_full, up_full = side_by_side((gate_weight, up_weight), "sp", 0, 1)
    down_full = lax.all_gather(down_weight, "sp", axis=1, tiled=True)
    seg_rows = queries.shape[0]
    head_count = key_bias.shape[0]
    head_width = queries.shape[1] // head_count
    sp_count = lax.axis_size("sp")
    token_place = lax.axis_index("sp")
    query_heads = queries.reshape(seg_rows, head_count, head_width)
    query_pos = token_place * seg_rows + lax.iota(jnp.int32, seg_rows)
    start_carry = (
        jnp.zeros((seg_rows, head_count, head_width), jnp.float32),
        jnp.zeros((head_count, seg_rows), jnp.float32),
    )
    carry = stick_block(
        start_carry, query_heads, key_rows, value_rows, key_bias, query_pos, token_place * seg_rows
    )
    all_keys, all_values, all_bias = turned_gather(
        (key_rows, value_rows, key_bias), "sp", (0, 0, 1)
    )

    def visit(hop_index, carry_now):
        source = jnp.maximum(token_place - hop_index, 0)
        begin = source * seg_rows

        def attend(current):
            key_block = lax.dynamic_slice_in_dim(all_keys, begin, seg_rows, 0)
            value_block = lax.dynamic_slice_in_dim(all_values, begin, seg_rows, 0)
            bias_block = lax.dynamic_slice_in_dim(all_bias, begin, seg_rows, 1)
            return stick_block(
                current,
                query_heads,
                key_block,
                value_block,
                bias_block,
                query_pos,
                (token_place - hop_index) * seg_rows,
            )

        return lax.cond(token_place >= hop_index, attend, lambda current: current, carry_now)

    carry = lax.fori_loop(1, sp_count, visit, carry)
    attended = carry[0].reshape(seg_rows, head_count * head_width).astype(jnp.bfloat16)
    own_rows = seg_rows // lax.axis_size("tp")
    own_start = lax.axis_index("tp") * own_rows
    mixed = sum_at_owner(
        jnp.dot(attended, out_weight, preferred_element_type=jnp.float32).astype(jnp.bfloat16),
        "tp",
        0,
    )
    own_residual = lax.dynamic_slice_in_dim(residual, own_start, own_rows, 0)
    middle = (own_residual.astype(jnp.float32) + mixed).astype(jnp.bfloat16)
    middle_wide = middle.astype(jnp.float32)
    normed_all = collect(normalize(middle_wide, norm_gain), "tp", 0)
    gate_pre = jnp.dot(normed_all, gate_full, preferred_element_type=jnp.float32)
    up_pre = jnp.dot(normed_all, up_full, preferred_element_type=jnp.float32)
    hidden = (jax.nn.silu(gate_pre) * up_pre).astype(jnp.bfloat16)
    down_terms = jnp.dot(hidden, down_full, preferred_element_type=jnp.float32)
    down_sum = sum_at_owner(down_terms.astype(jnp.bfloat16), "tp", 0)
    own_out = (middle_wide + down_sum).astype(jnp.bfloat16)
    return collect(own_out, "tp", 0)


def solution(mesh):
    in_specs = (
        P(("grp", "sp"), "tp"),
        P(("grp", "sp"), "tp"),
        P(("grp", "sp"), "tp"),
        P("tp", ("grp", "sp")),
        P(("grp", "sp"), None),
        P("tp", None),
        P(),
        P("sp", "tp"),
        P("sp", "tp"),
        P("tp", "sp"),
    )
    out_specs = P(("grp", "sp"), None)
    return jax.shard_map(body, mesh=mesh, in_specs=in_specs, out_specs=out_specs, check_vma=False)
```

profile of v0, /device:TPU:40, one launch (start us, length us, event | category | flops | bytes accessed | tf_op | source)
XLA Modules:
  0.0 273.2 jit_solution(14697455399693322357)
XLA Ops:
  6.5 0.0 copy-start
  6.6 0.0 all-gather.4.cloned.1.call-start
  6.6 0.9 copy.20
  7.5 0.9 copy.21
  8.4 1.3 pad_maximum_fusion.1
  9.7 0.1 all-gather.4.cloned.1.call-update
  9.7 0.1 all-gather.6.cloned.1.call-start
  9.8 1.6 pad_maximum_fusion
  11.4 0.1 all-gather.6.cloned.1.call-update
  11.5 0.1 all-gather.8.cloned.1.call-start
  11.6 0.7 all-gather.8.cloned.1.call-update
  12.3 0.7 convert_element_type.61
  13.0 0.9 copy.19
  13.8 0.1 compare_and_fusion.1
  14.0 0.2 fusion.48
  14.2 0.1 fusion.51
  14.3 2.2 reduce_window_sum.17
  16.5 0.3 convolution_bitcast_fusion.1
  16.8 77.8 %all-gather.4.cloned.1.call-done = bf16[4096,258]{0,1:T(8,128)(2,1)} async-done(((bf16[128,258]{0,1:T(8,128)(2,1)}), bf16[4096,258]{0,1:T(8,128)(2,1)}) %all-gather.4.cloned.1.call-update) | async-done | bytes 2113552 | tf_op jit(solution)/shard_map/all_gather | solution.py:22
  94.7 0.8 slice_bitcast_fusion
  95.5 1.7 fusion.52
  97.2 0.0 copy-start.1
  97.2 1.6 while.16
  98.9 0.0 copy-done
  98.9 1.1 convolution_convert_fusion.1
  100.0 4.3 %all-to-all-start = ((bf16[4,32,2048]{2,1,0:T(8,128)(2,1)}), bf16[4,32,2048]{2,1,0:T(8,128)(2,1)S(1)}, u32[]{:S(2)}, u32[]{:S(2)}) async-start(bf16[4,32,2048]{2,1,0:T(8,128)(2,1)} %bitcast.11), calls=%async_computation | async-start | bytes 1048576 | tf_op jit(solution)/shard_map/all_to_all | solution.py:40
  104.3 0.0 copy-done.1
  104.3 8.8 %all-to-all-done = bf16[4,32,2048]{2,1,0:T(8,128)(2,1)S(1)} async-done(((bf16[4,32,2048]{2,1,0:T(8,128)(2,1)}), bf16[4,32,2048]{2,1,0:T(8,128)(2,1)S(1)}, u32[]{:S(2)}, u32[]{:S(2)}) %all-to-all-start) | async-done | bytes 524320 | tf_op jit(solution)/shard_map/all_to_all | solution.py:40
  113.1 0.1 convert_reduce_fusion.1
  113.2 1.1 fusion.36
  114.3 0.1 fusion.38
  114.4 12.4 %all_to_all.20 = bf16[4,32,2048]{2,1,0:T(8,128)(2,1)S(1)} all-to-all(bf16[4,32,2048]{2,1,0:T(8,128)(2,1)S(1)} %broadcast_in_dim.46), channel_id=1, replica_groups=mesh['grp'=2,'sp'=32,'tp'=4] {'tp'}, dimensions={0} | all-to-all | bytes 1048576 | tf_op jit(solution)/shard_map/all_to_all | solution.py:52
  126.9 40.2 %all-gather.6.cloned.1.call-done = bf16[2048,1536]{1,0:T(8,128)(2,1)} async-done(((bf16[64,1536]{1,0:T(8,128)(2,1)}), bf16[2048,1536]{1,0:T(8,128)(2,1)}) %all-gather.6.cloned.1.call-update) | async-done | bytes 6291472 | tf_op jit(solution)/shard_map/all_gather | solution.py:11
  167.1 2.5 fusion.20
  169.6 66.3 %all-gather.8.cloned.1.call-done = bf16[768,2048]{0,1:T(8,128)(2,1)} async-done(((bf16[768,64]{0,1:T(8,128)(2,1)}), bf16[768,2048]{0,1:T(8,128)(2,1)}) %all-gather.8.cloned.1.call-update) | async-done | bytes 3145744 | tf_op jit(solution)/shard_map/all_gather | solution.py:104
  235.8 4.5 %convolution_convert_fusion = bf16[128,2048]{1,0:T(8,128)(2,1)S(1)} fusion(bf16[768,2048]{0,1:T(8,128)(2,1)} %all-gather.8.cloned.1.call-done, bf16[128,2048]{1,0:T(8,128)(2,1)S(1)} %bitcast.36, bf16[2048,1536]{1,0:T(8,128)(2,1)} %all-gather.6.cloned.1.call-done, f32[128,768]{1,0:T(8,128)S(1)} %fusion.20), kind=kOutput, calls=%fused_computation.30 | convolution fusion | flops 806158336 | bytes 7733248 | tf_op jit(solution)/shard_map/dot_general | solution.py:159
  240.3 13.9 %all_to_all.21 = bf16[4,32,2048]{2,1,0:T(8,128)(2,1)S(1)} all-to-all(bf16[4,32,2048]{2,1,0:T(8,128)(2,1)S(1)} %bitcast.37), channel_id=1, replica_groups=mesh['grp'=2,'sp'=32,'tp'=4] {'tp'}, dimensions={0} | all-to-all | bytes 1048576 | tf_op jit(solution)/shard_map/all_to_all | solution.py:40
  254.3 0.1 convert_reduce_fusion
  254.4 11.4 %all_to_all.22 = bf16[4,32,2048]{2,1,0:T(8,128)(2,1)S(1)} all-to-all(bf16[4,32,2048]{2,1,0:T(8,128)(2,1)S(1)} %broadcast_in_dim.47), channel_id=1, replica_groups=mesh['grp'=2,'sp'=32,'tp'=4] {'tp'}, dimensions={0} | all-to-all | bytes 1048576 | tf_op jit(solution)/shard_map/all_to_all | solution.py:52
  265.9 0.8 copy.41
  (70 shorter events, 0.7 us)
Async XLA Ops:
  6.5 92.3 %copy-start = (bf16[128,2048]{1,0:T(8,128)(2,1)S(1)}, bf16[128,2048]{1,0:T(8,128)(2,1)}, u32[]{:S(2)}) copy-start(bf16[128,2048]{1,0:T(8,128)(2,1)} %param.19) | copy-start | bytes 1572868
  6.6 88.1 %all-gather.4.cloned.1.call-start = ((), (), s32[]{:S(2)}) async-start(), calls=%async_computation.4 | async-start | bytes 2230272 | tf_op jit(solution)/shard_map/all_gather | solution.py:22
  9.7 157.4 %all-gather.6.cloned.1.call-start = ((), (), s32[]{:S(2)}) async-start(), calls=%async_computation.5 | async-start | bytes 6488064 | tf_op jit(solution)/shard_map/all_gather | solution.py:11
  11.5 224.3 %all-gather.8.cloned.1.call-start = ((), (), s32[]{:S(2)}) async-start(), calls=%async_computation.6 | async-start | bytes 3244032 | tf_op jit(solution)/shard_map/all_gather | solution.py:104
  97.2 7.1 %copy-start.1 = (bf16[2048]{0:T(1024)(128)(2,1)S(1)}, bf16[2048]{0:T(1024)(128)(2,1)}, u32[]{:S(2)}) copy-start(bf16[2048]{0:T(1024)(128)(2,1)} %param.20) | copy-start | bytes 12292
  100.0 13.1 %all-to-all-start = ((bf16[4,32,2048]{2,1,0:T(8,128)(2,1)}), bf16[4,32,2048]{2,1,0:T(8,128)(2,1)S(1)}, u32[]{:S(2)}, u32[]{:S(2)}) async-start(bf16[4,32,2048]{2,1,0:T(8,128)(2,1)} %bitcast.11), calls=%async_computation | async-start | bytes 1048576 | tf_op jit(solution)/shard_map/all_to_all | solution.py:40
Sparse Core Ops, SparseCore 0:
  9.8 84.7 all-gather.3
  96.5 70.5 all-gather.5
  168.9 66.8 all-gather.7
where the time goes:
time: 274 us; the launch traced here: 273 us
  waiting for transfers between devices  194 us (71%)
  blocking collectives  37.8 us (14%)
  between operations  13.3 us (5%)
  matrix products  8.63 us (3%)
  other arithmetic  7.43 us (3%)
  local copies, waits for them, and re-layouts  6.15 us (2%)
  starting transfers between devices  4.39 us (2%)
    all_gather x1, waiting for transfers between devices, turned_gather(): out = lax.all_gather(both, axis, axis=0, tiled=True)  77.8 us
    all_gather x1, waiting for transfers between devices, body(): down_full = lax.all_gather(down_weight, 'sp', axis=1, tiled=True)  66.3 us
    all_gather x1, waiting for transfers between devices, side_by_side(): out, at, done = (lax.all_gather(both, axis, axis=dim, tiled=True), 0, [])  40.2 us
    all_to_all x2, blocking collectives, sent_to_all(): return lax.all_to_all(copies, axis, split_axis=0, concat_axis=0, tiled=True)  23.9 us
    all_to_all x1, blocking collectives, sum_at_owner(): lax.all_to_all(cut_along(value, dim, length), axis, 0, 0, tiled=True)  13.9 us
    all_to_all x1, waiting for transfers between devices, sum_at_owner(): lax.all_to_all(cut_along(value, dim, length), axis, 0, 0, tiled=True)  8.84 us
  transfers between devices with their start and end apart: 4, of which 4 were waited for; matrix products, arithmetic and copies ran while one was open for 5% of the time, Pallas kernels for 0%

commit v1 on v0

--- a/solution.py
+++ b/solution.py
@@ -101,7 +101,9 @@
     down_weight,
 ):
     gate_full, up_full = side_by_side((gate_weight, up_weight), "sp", 0, 1)
-    down_full = lax.all_gather(down_weight, "sp", axis=1, tiled=True)
+    f_next = jnp.stack([down_weight for _ in range(lax.axis_size("sp"))])
+    view_out = lax.all_to_all(f_next, "sp", 0, 0)
+    down_full = jnp.concatenate(view_out, axis=1)
     seg_rows = queries.shape[0]
     head_count = key_bias.shape[0]
     head_width = queries.shape[1] // head_count

time: 274 us -> 438 us (1.60)
  starting transfers between devices: 4.39 us -> 104 us
  waiting for transfers between devices: 194 us -> 264 us
  blocking collectives: 37.8 us -> 29.1 us
    all_gather x1, waiting for transfers between devices: 40.2 us -> 161 us  [side_by_side(): out, at, done = (lax.all_gather(both, axis, axis=dim, tiled=True), 0, [])]
    all_to_all x0 -> x2, starting transfers between devices: none -> 100 us  [the longest x1 96.4 us: body(): view_out = lax.all_to_all(f_next, 'sp', 0, 0)]
    all_gather x1 -> x0, waiting for transfers between devices: 66.3 us -> none  [body(): down_full = lax.all_gather(down_weight, 'sp', axis=1, tiled=True)]
    all_to_all x0 -> x2, waiting for transfers between devices: none -> 13.5 us  [the longest x1 9.06 us: sent_to_all(): return lax.all_to_all(copies, axis, split_axis=0, concat_axis=0, tiled=True)]
    all_to_all x2 -> x1, blocking collectives: 23.9 us -> 11 us  [sent_to_all(): return lax.all_to_all(copies, axis, split_axis=0, concat_axis=0, tiled=True)]
  transfers between devices with their start and end apart: 4 -> 5, of which waited for: 4 -> 5; matrix products, arithmetic and copies ran while one was open for 5% -> 2% of each run, Pallas kernels for 0% -> 0%
where the time goes in v1:
time: 438 us; the launch traced here: 437 us
  waiting for transfers between devices  264 us (60%)
  starting transfers between devices  104 us (24%)
  blocking collectives  29.1 us (7%)
  between operations  13.6 us (3%)
  local copies, waits for them, and re-layouts  8.96 us (2%)
  matrix products  8.67 us (2%)
  other arithmetic  6.47 us (1%)
    all_gather x1, waiting for transfers between devices, side_by_side(): out, at, done = (lax.all_gather(both, axis, axis=dim, tiled=True), 0, [])  161 us
    all_to_all x1, starting transfers between devices, body(): view_out = lax.all_to_all(f_next, 'sp', 0, 0)  96.4 us
    all_gather x1, waiting for transfers between devices, turned_gather(): out = lax.all_gather(both, axis, axis=0, tiled=True)  80.4 us
    all_to_all x1, blocking collectives, sum_at_owner(): lax.all_to_all(cut_along(value, dim, length), axis, 0, 0, tiled=True)  18.1 us
    all_to_all x1, blocking collectives, sent_to_all(): return lax.all_to_all(copies, axis, split_axis=0, concat_axis=0, tiled=True)  11 us
    all_to_all x1, waiting for transfers between devices, sent_to_all(): return lax.all_to_all(copies, axis, split_axis=0, concat_axis=0, tiled=True)  9.06 us
    all_to_all x1, waiting for transfers between devices, sum_at_owner(): lax.all_to_all(cut_along(value, dim, length), axis, 0, 0, tiled=True)  8.85 us
  transfers between devices with their start and end apart: 5, of which 5 were waited for; matrix products, arithmetic and copies ran while one was open for 2% of the time, Pallas kernels for 0%

profile of v1, /device:TPU:40, one launch (start us, length us, event | category | flops | bytes accessed | tf_op | source)
XLA Modules:
  0.0 437.0 jit_solution(13688144661076011974)
XLA Ops:
  6.5 0.0 copy-start
  6.6 0.0 all-gather.3.cloned.1.call-start
  6.6 0.9 copy.22
  7.5 0.9 copy.21
  8.4 1.3 pad_maximum_fusion.1
  9.7 0.1 all-gather.3.cloned.1.call-update
  9.7 0.7 convert_element_type.61
  10.4 0.9 copy.20
  11.3 0.1 compare_and_fusion.1
  11.4 0.2 fusion.48
  11.6 0.1 fusion.51
  11.7 2.2 reduce_window_sum.17
  13.9 0.3 convolution_bitcast_fusion.1
  14.3 80.4 %all-gather.3.cloned.1.call-done = bf16[4096,258]{0,1:T(8,128)(2,1)} async-done(((bf16[128,258]{0,1:T(8,128)(2,1)}), bf16[4096,258]{0,1:T(8,128)(2,1)}) %all-gather.3.cloned.1.call-update) | async-done | bytes 2113552 | tf_op jit(solution)/shard_map/all_gather | solution.py:22
  94.7 1.7 fusion.52
  96.3 0.9 slice_bitcast_fusion
  97.2 0.0 copy-start.4
  97.2 1.6 while.16
  98.9 0.0 copy-start.2
  98.9 0.0 copy-start.3
  98.9 0.0 copy-start.1
  98.9 0.0 copy-done
  98.9 1.1 convolution_convert_fusion.1
  100.0 4.3 all-to-all-start
  104.3 0.0 copy-done.4
  104.3 8.8 %all-to-all-done = bf16[4,32,2048]{2,1,0:T(8,128)(2,1)S(1)} async-done(((bf16[4,32,2048]{2,1,0:T(8,128)(2,1)}), bf16[4,32,2048]{2,1,0:T(8,128)(2,1)S(1)}, u32[]{:S(2)}, u32[]{:S(2)}) %all-to-all-start) | async-done | bytes 524320 | tf_op jit(solution)/shard_map/all_to_all | solution.py:40
  113.1 0.1 convert_reduce_fusion.1
  113.2 1.1 fusion.36
  114.3 0.1 fusion.38
  114.4 0.8 broadcast_in_dim.46
  115.3 3.6 all-to-all-start.1
  118.8 0.1 all-gather.5.cloned.1.call-start
  118.9 0.0 copy-done.2
  118.9 0.0 copy-done.3
  118.9 0.7 pad_maximum_fusion
  119.6 0.1 all-gather.5.cloned.1.call-update
  119.7 9.1 %all-to-all-done.1 = bf16[4,32,2048]{2,1,0:T(8,128)(2,1)S(1)} async-done(((bf16[4,32,2048]{2,1,0:T(8,128)(2,1)}), bf16[4,32,2048]{2,1,0:T(8,128)(2,1)S(1)}, u32[]{:S(2)}, u32[]{:S(2)}) %all-to-all-start.1) | async-done | bytes 524320 | tf_op jit(solution)/shard_map/all_to_all | solution.py:52
  128.7 0.0 copy-done.1
  128.7 2.0 stack.2
  130.7 96.4 %all-to-all-start.2 = ((bf16[32,768,64]{1,2,0:T(8,128)(2,1)}), bf16[32,768,64]{1,2,0:T(8,128)(2,1)}, u32[]{:S(2)}, u32[]{:S(2)}) async-start(bf16[32,768,64]{1,2,0:T(8,128)(2,1)} %stack.2), calls=%async_computation.2 | async-start | bytes 6291456 | tf_op jit(solution)/shard_map/all_to_all | solution.py:105
  227.1 161.5 %all-gather.5.cloned.1.call-done = bf16[2048,1536]{1,0:T(8,128)(2,1)} async-done(((bf16[64,1536]{1,0:T(8,128)(2,1)}), bf16[2048,1536]{1,0:T(8,128)(2,1)}) %all-gather.5.cloned.1.call-update) | async-done | bytes 6291472 | tf_op jit(solution)/shard_map/all_gather | solution.py:11
  388.6 2.5 fusion.20
  391.1 4.4 %all-to-all-done.2 = bf16[32,768,64]{1,2,0:T(8,128)(2,1)} async-done(((bf16[32,768,64]{1,2,0:T(8,128)(2,1)}), bf16[32,768,64]{1,2,0:T(8,128)(2,1)}, u32[]{:S(2)}, u32[]{:S(2)}) %all-to-all-start.2) | async-done | bytes 3145760 | tf_op jit(solution)/shard_map/all_to_all | solution.py:105
  395.5 4.5 %convolution_convert_fusion = bf16[128,2048]{1,0:T(8,128)(2,1)S(1)} fusion(bf16[768,2048]{0,1:T(8,128)(2,1)} %bitcast.14, bf16[128,2048]{1,0:T(8,128)(2,1)S(1)} %bitcast.39, bf16[2048,1536]{1,0:T(8,128)(2,1)} %all-gather.5.cloned.1.call-done, f32[128,768]{1,0:T(8,128)S(1)} %fusion.20), kind=kOutput, calls=%fused_computation.30 | convolution fusion | flops 806158336 | bytes 7733248 | tf_op jit(solution)/shard_map/dot_general | solution.py:161
  400.1 18.1 %all_to_all.25 = bf16[4,32,2048]{2,1,0:T(8,128)(2,1)S(1)} all-to-all(bf16[4,32,2048]{2,1,0:T(8,128)(2,1)S(1)} %bitcast.40), channel_id=1, replica_groups=mesh['grp'=2,'sp'=32,'tp'=4] {'tp'}, dimensions={0} | all-to-all | bytes 1048576 | tf_op jit(solution)/shard_map/all_to_all | solution.py:40
  418.1 0.1 convert_reduce_fusion
  418.3 11.0 %all_to_all.26 = bf16[4,32,2048]{2,1,0:T(8,128)(2,1)S(1)} all-to-all(bf16[4,32,2048]{2,1,0:T(8,128)(2,1)S(1)} %broadcast_in_dim.47), channel_id=1, replica_groups=mesh['grp'=2,'sp'=32,'tp'=4] {'tp'}, dimensions={0} | all-to-all | bytes 1048576 | tf_op jit(solution)/shard_map/all_to_all | solution.py:52
  429.3 0.8 copy.42
  (69 shorter events, 0.6 us)
Async XLA Ops:
  6.5 92.4 %copy-start = (bf16[128,2048]{1,0:T(8,128)(2,1)S(1)}, bf16[128,2048]{1,0:T(8,128)(2,1)}, u32[]{:S(2)}) copy-start(bf16[128,2048]{1,0:T(8,128)(2,1)} %param.19) | copy-start | bytes 1572868
  6.6 88.1 %all-gather.3.cloned.1.call-start = ((), (), s32[]{:S(2)}) async-start(), calls=%async_computation.5 | async-start | bytes 2230272 | tf_op jit(solution)/shard_map/all_gather | solution.py:22
  97.2 7.1 %copy-start.4 = (bf16[2048]{0:T(1024)(128)(2,1)S(1)}, bf16[2048]{0:T(1024)(128)(2,1)}, u32[]{:S(2)}) copy-start(bf16[2048]{0:T(1024)(128)(2,1)} %param.20) | copy-start | bytes 12292
  98.9 20.1 %copy-start.2 = (bf16[64,768]{1,0:T(8,128)(2,1)S(1)}, bf16[64,768]{1,0:T(8,128)(2,1)}, u32[]{:S(2)}) copy-start(bf16[64,768]{1,0:T(8,128)(2,1)} %param.22) | copy-start | bytes 294916
  98.9 20.0 %copy-start.3 = (bf16[64,768]{1,0:T(8,128)(2,1)S(1)}, bf16[64,768]{1,0:T(8,128)(2,1)}, u32[]{:S(2)}) copy-start(bf16[64,768]{1,0:T(8,128)(2,1)} %param.21) | copy-start | bytes 294916
  98.9 29.9 %copy-start.1 = (bf16[768,64]{0,1:T(8,128)(2,1)S(1)}, bf16[768,64]{0,1:T(8,128)(2,1)}, u32[]{:S(2)}) copy-start(bf16[768,64]{0,1:T(8,128)(2,1)} %param.23) | copy-start | bytes 294916
  100.0 13.1 %all-to-all-start = ((bf16[4,32,2048]{2,1,0:T(8,128)(2,1)}), bf16[4,32,2048]{2,1,0:T(8,128)(2,1)S(1)}, u32[]{:S(2)}, u32[]{:S(2)}) async-start(bf16[4,32,2048]{2,1,0:T(8,128)(2,1)} %bitcast.11), calls=%async_computation | async-start | bytes 1048576 | tf_op jit(solution)/shard_map/all_to_all | solution.py:40
  115.3 13.5 %all-to-all-start.1 = ((bf16[4,32,2048]{2,1,0:T(8,128)(2,1)}), bf16[4,32,2048]{2,1,0:T(8,128)(2,1)S(1)}, u32[]{:S(2)}, u32[]{:S(2)}) async-start(bf16[4,32,2048]{2,1,0:T(8,128)(2,1)} %broadcast_in_dim.46), calls=%async_computation.1 | async-start | bytes 1048576 | tf_op jit(solution)/shard_map/all_to_all | solution.py:52
  118.8 269.8 %all-gather.5.cloned.1.call-start = ((), (), s32[]{:S(2)}) async-start(), calls=%async_computation.6 | async-start | bytes 6488064 | tf_op jit(solution)/shard_map/all_gather | solution.py:11
  130.7 264.8 %all-to-all-start.2 = ((bf16[32,768,64]{1,2,0:T(8,128)(2,1)}), bf16[32,768,64]{1,2,0:T(8,128)(2,1)}, u32[]{:S(2)}, u32[]{:S(2)}) async-start(bf16[32,768,64]{1,2,0:T(8,128)(2,1)} %stack.2), calls=%async_computation.2 | async-start | bytes 6291456 | tf_op jit(solution)/shard_map/all_to_all | solution.py:105
Sparse Core Ops, SparseCore 0:
  9.8 84.7 all-gather.2
  121.5 267.0 all-gather.4
